TPU v7x, 256 devices: a 4x2x16 block of a 4x16x16 slice. The times are simulated.
256 devices in a mesh: grp: 2 (over y), fs: 32 (over z, core), tp: 4 (over x).
Axes of the slice: x: 4, y: 2, z: 16, core: 2. Of those that a mesh axis runs over, the one named last changes fastest.
The devices are a block of a 4x16x16 slice.
Arguments:
- prompt: bfloat16 [8, 1024, 2048], P(('grp', 'tp')), parts along dimension 0, may hold values from -6 to 6
- gate_first: float32 [2048, 5632], P('fs', 'tp'), may hold values from -0.125 to 0.125
- up_first: float32 [2048, 5632], P('fs', 'tp'), may hold values from -0.125 to 0.125
- down_first: float32 [5632, 2048], P('fs', 'tp'), may hold values from -0.3125 to 0.3125
- norm_gain: float32 [2048], replicated, may hold values from 0.1 to 1.9
- gate_second: float32 [2048, 5632], P('fs', 'tp'), may hold values from -0.125 to 0.125
- up_second: float32 [2048, 5632], P('fs', 'tp'), may hold values from -0.125 to 0.125
- down_second: float32 [5632, 2048], P('fs', 'tp'), may hold values from -0.3125 to 0.3125
Outputs:
- result: bfloat16 [8, 1024, 2048], P(('grp', 'tp'), 'fs'), parts along dimension 0
- gate_one: bfloat16 [4096, 5632], P('grp', 'fs'), parts along dimension 0
- up_one: bfloat16 [4096, 5632], P('grp', 'fs'), parts along dimension 0
- down_one: bfloat16 [5632, 4096], P('fs', 'grp'), parts along dimension 1
- gate_two: bfloat16 [4096, 5632], P('grp', 'fs'), parts along dimension 0
- up_two: bfloat16 [4096, 5632], P('grp', 'fs'), parts along dimension 0
- down_two: bfloat16 [5632, 4096], P('fs', 'grp'), parts along dimension 1
There are 2 independent parts, one for each index of `grp`. A program takes and returns all parts, laid end to end along the dimension named above; an argument that names none is the same for every part. Nothing has to cross between parts.
All inputs are finite; a program needn't handle non-finite values.
Results may differ from a plain program's by a relative error of at most 0.029.
Values may be sent and summed in bfloat16 or wider, within the bound.
A program may use at most 64 MiB of HBM per device.

v0:
```python
import jax
import jax.numpy as jnp
from jax import lax
from jax.sharding import Mesh
from jax.sharding import PartitionSpec as P

FS = ("fs_0", "fs_1")
norm_eps = 1e-05
deep_alpha = 2.0**0.25
half_step = 0.5


def reduced_to_own(pieces, axes, sequence):
    inside = pieces.shape[1:]
    pieces = pieces.reshape(*(lax.axis_size(a) for a in axes), *inside)
    pieces = jnp.moveaxis(pieces, sequence, range(len(axes))).reshape(-1, *inside)
    for k in sequence:
        pieces = lax.psum_scatter(pieces, axes[k], scatter_dimension=0, tiled=True)
    return pieces[0]


def cut_along(value, dim, size):
    before, after = (value.shape[:dim], value.shape[dim + 1 :])
    return jnp.moveaxis(value.reshape(*before, size, -1, *after), dim, 0)


def scatter_axes(value, axes, sequence, dim):
    size = lax.axis_size(axes)
    return reduced_to_own(cut_along(value, dim, size), axes, sequence)


def plain_norm(values):
    row_mean = jnp.mean(values, axis=-1, keepdims=True)
    centred = values - row_mean
    variance = jnp.mean(centred * centred, axis=-1, keepdims=True)
    return centred * lax.rsqrt(variance + norm_eps)


def gated_hidden(inputs, gate_proj, up_proj):
    gate_act = jnp.dot(inputs, gate_proj, preferred_element_type=jnp.float32)
    up_act = jnp.dot(inputs, up_proj, preferred_element_type=jnp.float32)
    return (jax.nn.silu(gate_act) * up_act).astype(jnp.bfloat16)


def relay_weights(gate_proj, up_proj, down_proj):
    gate_rows, up_rows, down_mine = (
        lax.all_gather(gate_proj, "tp", axis=1, tiled=True),
        lax.all_gather(up_proj, "tp", axis=1, tiled=True),
        lax.all_gather(down_proj, "tp", axis=1, tiled=True),
    )
    gate_mine, up_mine = (
        lax.all_to_all(gate_rows, FS, split_axis=1, concat_axis=0, tiled=True),
        lax.all_to_all(up_rows, FS, split_axis=1, concat_axis=0, tiled=True),
    )
    return (gate_mine, up_mine, down_mine)


def row_terms(hidden, down_proj):
    return jnp.dot(hidden, down_proj, preferred_element_type=jnp.float32)


def body(prompt, gate_first, up_first, down_first, norm_gain, gate_second, up_second, down_second):
    fs_index = lax.axis_index(FS)
    row_block = gate_first.shape[0]
    gain_rows = lax.dynamic_slice_in_dim(norm_gain, fs_index * row_block, row_block, 0)
    gate_one, up_one, down_one = relay_weights(
        gate_first.astype(jnp.bfloat16),
        up_first.astype(jnp.bfloat16),
        down_first.astype(jnp.bfloat16),
    )
    gate_two, up_two, down_two = relay_weights(
        (gain_rows[:, None] * gate_second).astype(jnp.bfloat16),
        (gain_rows[:, None] * up_second).astype(jnp.bfloat16),
        down_second.astype(jnp.bfloat16),
    )
    tokens = prompt.reshape(-1, prompt.shape[-1])
    own_count = tokens.shape[0] // lax.axis_size(FS)
    own_first = fs_index * own_count
    hidden_one = gated_hidden(tokens, gate_one, up_one)
    own_tokens = lax.dynamic_slice_in_dim(tokens, own_first, own_count, 0)
    ffn_one = scatter_axes(
        row_terms(hidden_one, down_one).astype(jnp.bfloat16), FS, (1, 0), 0
    ).astype(jnp.float32)
    normed_own = plain_norm(
        deep_alpha * own_tokens.astype(jnp.float32) + half_step * ffn_one
    ).astype(jnp.bfloat16)
    hidden_two = gated_hidden(lax.all_gather(normed_own, FS, axis=0, tiled=True), gate_two, up_two)
    ffn_two = scatter_axes(
        row_terms(hidden_two, down_two).astype(jnp.bfloat16), FS, (1, 0), 0
    ).astype(jnp.float32)
    residual_two = deep_alpha * norm_gain * normed_own.astype(jnp.float32)
    result = plain_norm(residual_two + half_step * ffn_two).astype(jnp.bfloat16)
    return (
        result.reshape(1, result.shape[0], result.shape[-1]),
        gate_one,
        up_one,
        down_one,
        gate_two,
        up_two,
        down_two,
    )


def solution(mesh):
    torus = Mesh(
        mesh.devices.reshape(mesh.shape["grp"], 16, 2, mesh.shape["tp"]),
        ("grp", "fs_0", "fs_1", "tp"),
    )
    placed = (
        P(("grp", "tp"), None, None),
        P(FS, "tp"),
        P(FS, "tp"),
        P(FS, "tp"),
        P(),
        P(FS, "tp"),
        P(FS, "tp"),
        P(FS, "tp"),
    )
    return jax.shard_map(
        body,
        mesh=torus,
        in_specs=placed,
        out_specs=(
            P(("grp", "tp"), FS, None),
            P("grp", FS),
            P("grp", FS),
            P(FS, "grp"),
            P("grp", FS),
            P("grp", FS),
            P(FS, "grp"),
        ),
        check_vma=False,
    )
```

profile of v0, /device:TPU:34, one launch (start us, length us, event | category | flops | bytes accessed | tf_op | source)
XLA Modules:
  0.0 540.0 jit_solution(11706451847986128299)
XLA Ops:
  8.2 29.5 %all_gather.21 = bf16[64,5632]{1,0:T(8,128)(2,1)S(1)} all-gather(bf16[64,1408]{1,0:T(8,128)(2,1)S(1)} %convert_element_type.62), channel_id=1, replica_groups=mesh['grp'=2,'fs_0'=16,'fs_1'=2,'tp'=4] {'tp'}, dimensions={1}, use_global_device_ids=true | all-gather | bytes 901120 | tf_op jit(solution)/shard_map/all_gather | solution.py:47
  41.4 9.7 %all-to-all-start = ((bf16[64,32,176]{2,0,1:T(8,128)(2,1)}), bf16[64,32,176]{2,0,1:T(8,128)(2,1)S(1)}, u32[]{:S(2)}, u32[]{:S(2)}) async-start(bf16[64,32,176]{2,0,1:T(8,128)(2,1)} %copy.21), calls=%async_computation | async-start | bytes 2097152 | tf_op jit(solution)/shard_map/all_to_all | solution.py:52
  51.2 14.4 %all_gather.22 = bf16[64,5632]{1,0:T(8,128)(2,1)S(1)} all-gather(bf16[64,1408]{1,0:T(8,128)(2,1)S(1)} %convert_element_type.63), channel_id=1, replica_groups=mesh['grp'=2,'fs_0'=16,'fs_1'=2,'tp'=4] {'tp'}, dimensions={1}, use_global_device_ids=true | all-gather | bytes 901120 | tf_op jit(solution)/shard_map/all_gather | solution.py:48
  69.1 37.3 %all-to-all-done = bf16[64,32,176]{2,0,1:T(8,128)(2,1)S(1)} async-done(((bf16[64,32,176]{2,0,1:T(8,128)(2,1)}), bf16[64,32,176]{2,0,1:T(8,128)(2,1)S(1)}, u32[]{:S(2)}, u32[]{:S(2)}) %all-to-all-start) | async-done | bytes 720928 | tf_op jit(solution)/shard_map/all_to_all | solution.py:52
  106.4 4.8 all-to-all-start.1
  111.4 14.2 %all_gather.23 = bf16[176,2048]{1,0:T(8,128)(2,1)S(1)} all-gather(bf16[176,512]{1,0:T(8,128)(2,1)S(1)} %convert_element_type.65), channel_id=1, replica_groups=mesh['grp'=2,'fs_0'=16,'fs_1'=2,'tp'=4] {'tp'}, dimensions={1}, use_global_device_ids=true | all-gather | bytes 901120 | tf_op jit(solution)/shard_map/all_gather | solution.py:49
  125.6 4.0 fusion.2
  129.6 37.3 %all-to-all-done.1 = bf16[64,32,176]{2,0,1:T(8,128)(2,1)S(1)} async-done(((bf16[64,32,176]{2,0,1:T(8,128)(2,1)}), bf16[64,32,176]{2,0,1:T(8,128)(2,1)S(1)}, u32[]{:S(2)}, u32[]{:S(2)}) %all-to-all-start.1) | async-done | bytes 720928 | tf_op jit(solution)/shard_map/all_to_all | solution.py:53
  167.0 7.0 %convolution_convert_fusion.1 = bf16[1024,2048]{1,0:T(8,128)(2,1)} fusion(bf16[176,2048]{1,0:T(8,128)(2,1)S(1)} %all_gather.23, bf16[2048,176]{1,0:T(8,128)(2,1)S(1)} %bitcast.57, bf16[1,1024,2048]{2,1,0:T(8,128)(2,1)} %param.8, f32[1024,176]{0,1:T(8,128)S(1)} %fusion.2), kind=kOutput, calls=%fused_computation.5 | convolution fusion | flops 1479573504 | bytes 10551296 | tf_op jit(solution)/shard_map/dot_general | solution.py:59
  173.9 4.7 copy.23
  178.8 12.5 %reduce-scatter.5.cloned.1.call-done = bf16[16,32,2048]{2,1,0:T(8,128)(2,1)} async-done(((bf16[32,32,2048]{2,1,0:T(8,128)(2,1)}), bf16[16,32,2048]{2,1,0:T(8,128)(2,1)}) %reduce-scatter.5.cloned.1.call-update) | async-done | bytes 2097168 | tf_op jit(solution)/shard_map/reduce_scatter | solution.py:18
  191.4 75.9 %reduce-scatter.7.cloned.1.call-done = bf16[1,32,2048]{2,1,0:T(8,128)(2,1)} async-done(((bf16[16,32,2048]{2,1,0:T(8,128)(2,1)}), bf16[1,32,2048]{2,1,0:T(8,128)(2,1)}) %reduce-scatter.7.cloned.1.call-update) | async-done | bytes 131088 | tf_op jit(solution)/shard_map/reduce_scatter | solution.py:18
  271.7 14.1 %all_gather.25 = bf16[64,5632]{1,0:T(8,128)(2,1)} all-gather(bf16[64,1408]{1,0:T(8,128)(2,1)S(1)} %get-tuple-element.14), channel_id=1, replica_groups=mesh['grp'=2,'fs_0'=16,'fs_1'=2,'tp'=4] {'tp'}, dimensions={1}, use_global_device_ids=true | all-gather | bytes 901120 | tf_op jit(solution)/shard_map/all_gather | solution.py:47
  290.4 9.7 %all-to-all-start.2 = ((bf16[64,32,176]{2,0,1:T(8,128)(2,1)}), bf16[64,32,176]{2,0,1:T(8,128)(2,1)S(1)}, u32[]{:S(2)}, u32[]{:S(2)}) async-start(bf16[64,32,176]{2,0,1:T(8,128)(2,1)} %copy.24), calls=%async_computation.4 | async-start | bytes 2097152 | tf_op jit(solution)/shard_map/all_to_all | solution.py:52
  300.1 14.3 %all_gather.26 = bf16[64,5632]{1,0:T(8,128)(2,1)} all-gather(bf16[64,1408]{1,0:T(8,128)(2,1)S(1)} %get-tuple-element.15), channel_id=1, replica_groups=mesh['grp'=2,'fs_0'=16,'fs_1'=2,'tp'=4] {'tp'}, dimensions={1}, use_global_device_ids=true | all-gather | bytes 901120 | tf_op jit(solution)/shard_map/all_gather | solution.py:48
  321.0 44.7 %all-to-all-done.2 = bf16[64,32,176]{2,0,1:T(8,128)(2,1)S(1)} async-done(((bf16[64,32,176]{2,0,1:T(8,128)(2,1)}), bf16[64,32,176]{2,0,1:T(8,128)(2,1)S(1)}, u32[]{:S(2)}, u32[]{:S(2)}) %all-to-all-start.2) | async-done | bytes 720928 | tf_op jit(solution)/shard_map/all_to_all | solution.py:52
  365.7 5.7 %all-to-all-start.3 = ((bf16[64,32,176]{2,0,1:T(8,128)(2,1)}), bf16[64,32,176]{2,0,1:T(8,128)(2,1)}, u32[]{:S(2)}, u32[]{:S(2)}) async-start(bf16[64,32,176]{2,0,1:T(8,128)(2,1)} %copy.25), calls=%async_computation.5 | async-start | bytes 2097152 | tf_op jit(solution)/shard_map/all_to_all | solution.py:53
  371.5 14.5 %all_gather.27 = bf16[176,2048]{1,0:T(8,128)(2,1)} all-gather(bf16[176,512]{1,0:T(8,128)(2,1)S(1)} %convert_element_type.74), channel_id=1, replica_groups=mesh['grp'=2,'fs_0'=16,'fs_1'=2,'tp'=4] {'tp'}, dimensions={1}, use_global_device_ids=true | all-gather | bytes 901120 | tf_op jit(solution)/shard_map/all_gather | solution.py:49
  386.0 4.6 fusion.29
  390.6 36.6 %all-to-all-done.3 = bf16[64,32,176]{2,0,1:T(8,128)(2,1)} async-done(((bf16[64,32,176]{2,0,1:T(8,128)(2,1)}), bf16[64,32,176]{2,0,1:T(8,128)(2,1)}, u32[]{:S(2)}, u32[]{:S(2)}) %all-to-all-start.3) | async-done | bytes 720928 | tf_op jit(solution)/shard_map/all_to_all | solution.py:53
  427.2 7.7 %convolution_convert_fusion = bf16[1024,2048]{1,0:T(8,128)(2,1)} fusion(bf16[176,2048]{1,0:T(8,128)(2,1)} %all_gather.27, bf16[1024,2048]{1,0:T(8,128)(2,1)} %all-gather.2.cloned.1.call-done, bf16[2048,176]{1,0:T(8,128)(2,1)} %bitcast.12, f32[1024,176]{0,1:T(8,128)} %fusion.29), kind=kOutput, calls=%fused_computation.4 | convolution fusion | flops 1479573504 | bytes 10551296 | tf_op jit(solution)/shard_map/dot_general | solution.py:59
  434.9 4.7 copy.26
  439.7 11.8 %reduce-scatter.9.cloned.1.call-done = bf16[16,32,2048]{2,1,0:T(8,128)(2,1)} async-done(((bf16[32,32,2048]{2,1,0:T(8,128)(2,1)}), bf16[16,32,2048]{2,1,0:T(8,128)(2,1)}) %reduce-scatter.9.cloned.1.call-update) | async-done | bytes 2097168 | tf_op jit(solution)/shard_map/reduce_scatter | solution.py:18
  457.6 70.1 %reduce-scatter.11.cloned.1.call-done = bf16[1,32,2048]{2,1,0:T(8,128)(2,1)} async-done(((bf16[16,32,2048]{2,1,0:T(8,128)(2,1)}), bf16[1,32,2048]{2,1,0:T(8,128)(2,1)}) %reduce-scatter.11.cloned.1.call-update) | async-done | bytes 131088 | tf_op jit(solution)/shard_map/reduce_scatter | solution.py:18
  (60 shorter events, 36.2 us)
Async XLA Ops:
  7.2 43.9 %copy-start.3 = (f32[64,1408]{1,0:T(8,128)S(1)}, f32[64,1408]{1,0:T(8,128)}, u32[]{:S(2)}) copy-start(f32[64,1408]{1,0:T(8,128)} %param.10) | copy-start | bytes 1081348
  41.4 65.0 %all-to-all-start = ((bf16[64,32,176]{2,0,1:T(8,128)(2,1)}), bf16[64,32,176]{2,0,1:T(8,128)(2,1)S(1)}, u32[]{:S(2)}, u32[]{:S(2)}) async-start(bf16[64,32,176]{2,0,1:T(8,128)(2,1)} %copy.21), calls=%async_computation | async-start | bytes 2097152 | tf_op jit(solution)/shard_map/all_to_all | solution.py:52
  51.1 60.2 %copy-start.4 = (f32[176,512]{1,0:T(8,128)S(1)}, f32[176,512]{1,0:T(8,128)}, u32[]{:S(2)}) copy-start(f32[176,512]{1,0:T(8,128)} %param.11) | copy-start | bytes 1081348
  106.4 60.6 %all-to-all-start.1 = ((bf16[64,32,176]{2,0,1:T(8,128)(2,1)}), bf16[64,32,176]{2,0,1:T(8,128)(2,1)S(1)}, u32[]{:S(2)}, u32[]{:S(2)}) async-start(bf16[64,32,176]{2,0,1:T(8,128)(2,1)} %copy.22), calls=%async_computation.1 | async-start | bytes 2097152 | tf_op jit(solution)/shard_map/all_to_all | solution.py:53
  111.3 80.0 %reduce-scatter.5.cloned.1.call-start = ((), (), s32[]{:S(2)}) async-start(), calls=%async_computation.8 | async-start | bytes 6291456 | tf_op jit(solution)/shard_map/reduce_scatter | solution.py:18
  125.6 41.4 %copy-start = (bf16[176,2048]{1,0:T(8,128)(2,1)}, bf16[176,2048]{1,0:T(8,128)(2,1)S(1)}, u32[]{:S(2)}) copy-start(bf16[176,2048]{1,0:T(8,128)(2,1)S(1)} %all_gather.23) | copy-start | bytes 2162692
  178.7 92.8 %copy-start.8 = (f32[2048]{0:T(1024)S(1)}, f32[2048]{0:T(1024)}, u32[]{:S(2)}) copy-start(f32[2048]{0:T(1024)} %param.12) | copy-start | bytes 24580
  178.7 92.9 %copy-start.6 = (f32[64,1408]{1,0:T(8,128)S(1)}, f32[64,1408]{1,0:T(8,128)}, u32[]{:S(2)}) copy-start(f32[64,1408]{1,0:T(8,128)} %param.13) | copy-start | bytes 1081348
  178.7 92.9 %copy-start.7 = (f32[64,1408]{1,0:T(8,128)S(1)}, f32[64,1408]{1,0:T(8,128)}, u32[]{:S(2)}) copy-start(f32[64,1408]{1,0:T(8,128)} %param.14) | copy-start | bytes 1081348
  178.7 88.6 %reduce-scatter.7.cloned.1.call-start = ((), (), s32[]{:S(2)}) async-start(), calls=%async_computation.9 | async-start | bytes 2228224 | tf_op jit(solution)/shard_map/reduce_scatter | solution.py:18
  191.3 194.7 %all-gather.2.cloned.1.call-start = ((), (), s32[]{:S(2)}) async-start(), calls=%async_computation.10 | async-start | bytes 4325376 | tf_op jit(solution)/shard_map/all_gather | solution.py:87
  290.4 75.3 %all-to-all-start.2 = ((bf16[64,32,176]{2,0,1:T(8,128)(2,1)}), bf16[64,32,176]{2,0,1:T(8,128)(2,1)S(1)}, u32[]{:S(2)}, u32[]{:S(2)}) async-start(bf16[64,32,176]{2,0,1:T(8,128)(2,1)} %copy.24), calls=%async_computation.4 | async-start | bytes 2097152 | tf_op jit(solution)/shard_map/all_to_all | solution.py:52
  314.4 57.1 %copy-start.5 = (f32[176,512]{1,0:T(8,128)S(1)}, f32[176,512]{1,0:T(8,128)}, u32[]{:S(2)}) copy-start(f32[176,512]{1,0:T(8,128)} %param.15) | copy-start | bytes 1081348
  365.7 61.5 %all-to-all-start.3 = ((bf16[64,32,176]{2,0,1:T(8,128)(2,1)}), bf16[64,32,176]{2,0,1:T(8,128)(2,1)}, u32[]{:S(2)}, u32[]{:S(2)}) async-start(bf16[64,32,176]{2,0,1:T(8,128)(2,1)} %copy.25), calls=%async_computation.5 | async-start | bytes 2097152 | tf_op jit(solution)/shard_map/all_to_all | solution.py:53
  371.4 80.1 %reduce-scatter.9.cloned.1.call-start = ((), (), s32[]{:S(2)}) async-start(), calls=%async_computation.11 | async-start | bytes 6291456 | tf_op jit(solution)/shard_map/reduce_scatter | solution.py:18
  439.7 87.9 %reduce-scatter.11.cloned.1.call-start = ((), (), s32[]{:S(2)}) async-start(), calls=%async_computation.12 | async-start | bytes 2228224 | tf_op jit(solution)/shard_map/reduce_scatter | solution.py:18
  452.9 78.9 %copy-start.1 = (bf16[176,2048]{1,0:T(8,128)(2,1)S(1)}, bf16[176,2048]{1,0:T(8,128)(2,1)}, u32[]{:S(2)}) copy-start(bf16[176,2048]{1,0:T(8,128)(2,1)} %copy-done) | copy-start | bytes 2162692
  452.9 79.8 %copy-start.2 = (bf16[176,2048]{1,0:T(8,128)(2,1)S(1)}, bf16[176,2048]{1,0:T(8,128)(2,1)}, u32[]{:S(2)}) copy-start(bf16[176,2048]{1,0:T(8,128)(2,1)} %all_gather.27) | copy-start | bytes 2162692
Sparse Core Ops, SparseCore 0:
  178.9 12.3 reduce-scatter.4
  193.8 73.4 reduce-scatter.6
  271.6 98.2 all-gather.1
  439.8 11.7 reduce-scatter.8
  454.0 73.5 reduce-scatter.10
where the time goes:
time: 541 us; the launch traced here: 540 us
  waiting for transfers between devices  326 us (60%)
  blocking collectives  101 us (19%)
  local copies, waits for them, and re-layouts  35.6 us (7%)
  starting transfers between devices  30.2 us (6%)
  matrix products  23.2 us (4%)
  between operations  14 us (3%)
  other arithmetic  9.45 us (2%)
    reduce_scatter x4, waiting for transfers between devices, reduced_to_own(): pieces = lax.psum_scatter(pieces, axes[k], scatter_dimension=0, tiled=True)  170 us
    all_to_all x2, waiting for transfers between devices, relay_weights(): lax.all_to_all(gate_rows, FS, split_axis=1, concat_axis=0, tiled=True)  82 us
    all_to_all x2, waiting for transfers between devices, relay_weights(): lax.all_to_all(up_rows, FS, split_axis=1, concat_axis=0, tiled=True)  73.9 us
    all_gather x2, blocking collectives, relay_weights(): lax.all_gather(gate_proj, 'tp', axis=1, tiled=True)  43.7 us
    all_gather x2, blocking collectives, relay_weights(): lax.all_gather(down_proj, 'tp', axis=1, tiled=True)  28.7 us
    all_gather x2, blocking collectives, relay_weights(): lax.all_gather(up_proj, 'tp', axis=1, tiled=True)  28.6 us
    all_to_all x2, starting transfers between devices, relay_weights(): lax.all_to_all(gate_rows, FS, split_axis=1, concat_axis=0, tiled=True)  19.4 us
    dot_general x2, matrix products, row_terms(): return jnp.dot(hidden, down_proj, preferred_element_type=jnp.float32)  14.6 us
  transfers between devices with their start and end apart: 9, of which 8 were waited for; matrix products, arithmetic and copies ran while one was open for 4% of the time, Pallas kernels for 0%

commit v1 on v0

--- a/solution.py
+++ b/solution.py
@@ -8,6 +8,28 @@
 norm_eps = 1e-05
 deep_alpha = 2.0**0.25
 half_step = 0.5
+
+
+def laid_out(parts, dim):
+    shape = list(parts.shape[1:])
+    shape[dim] *= parts.shape[0]
+    return jnp.moveaxis(parts, 0, dim).reshape(shape)
+
+
+def gather_around(x, axis, dim):
+    length = lax.axis_size(axis)
+    pairs = [(i, (i + 1) % length) for i in range(length)]
+    back = [(b, a) for a, b in pairs]
+    lower, upper = ([], [])
+    for step in range(length - 1):
+        if step % 2 == 0:
+            lower.append(lax.ppermute(lower[-1] if lower else x, axis, pairs))
+        else:
+            upper.append(lax.ppermute(upper[-1] if upper else x, axis, back))
+    pieces = jnp.stack([*lower[::-1], x, *upper])
+    shift = lax.axis_index(axis) - len(lower)
+    pieces = pieces[(jnp.arange(length) - shift) % length]
+    return laid_out(pieces, dim)
 
 
 def reduced_to_own(pieces, axes, sequence):
@@ -44,7 +66,7 @@
 
 def relay_weights(gate_proj, up_proj, down_proj):
     gate_rows, up_rows, down_mine = (
-        lax.all_gather(gate_proj, "tp", axis=1, tiled=True),
+        gather_around(gate_proj, "tp", 1),
         lax.all_gather(up_proj, "tp", axis=1, tiled=True),
         lax.all_gather(down_proj, "tp", axis=1, tiled=True),
     )

time: 541 us -> 539 us (level)
  blocking collectives: 101 us -> 56.8 us
  starting transfers between devices: 30.2 us -> 50.8 us
  waiting for transfers between devices: 326 us -> 344 us
    all_gather x2 -> x0, blocking collectives: 43.7 us -> none  [relay_weights(): lax.all_gather(gate_proj, 'tp', axis=1, tiled=True)]
    ppermute x0 -> x6, starting transfers between devices: none -> 23.1 us  [the longest x2 18.5 us: gather_around(): upper.append(lax.ppermute(upper[-1] if upper else x, axis, back))]
    ppermute x0 -> x6, waiting for transfers between devices: none -> 16.5 us  [the longest x4 16.5 us: gather_around(): lower.append(lax.ppermute(lower[-1] if lower else x, axis, pairs))]
  transfers between devices with their start and end apart: 9 -> 15, of which waited for: 8 -> 12; matrix products, arithmetic and copies ran while one was open for 4% -> 5% of each run, Pallas kernels for 0% -> 0%
where the time goes in v1:
time: 539 us; the launch traced here: 538 us
  waiting for transfers between devices  344 us (64%)
  blocking collectives  56.8 us (11%)
  starting transfers between devices  50.8 us (9%)
  local copies, waits for them, and re-layouts  38.1 us (7%)
  matrix products  23.2 us (4%)
  between operations  14.1 us (3%)
  other arithmetic  11.1 us (2%)
    reduce_scatter x4, waiting for transfers between devices, reduced_to_own(): pieces = lax.psum_scatter(pieces, axes[k], scatter_dimension=0, tiled=True)  172 us
    all_to_all x2, waiting for transfers between devices, relay_weights(): lax.all_to_all(gate_rows, FS, split_axis=1, concat_axis=0, tiled=True)  81.1 us
    all_to_all x2, waiting for transfers between devices, relay_weights(): lax.all_to_all(up_rows, FS, split_axis=1, concat_axis=0, tiled=True)  73.8 us
    all_gather x2, blocking collectives, relay_weights(): lax.all_gather(down_proj, 'tp', axis=1, tiled=True)  28.4 us
    all_gather x2, blocking collectives, relay_weights(): lax.all_gather(up_proj, 'tp', axis=1, tiled=True)  28.4 us
    ppermute x2, starting transfers between devices, gather_around(): upper.append(lax.ppermute(upper[-1] if upper else x, axis, back))  18.5 us
    all_to_all x2, starting transfers between devices, relay_weights(): lax.all_to_all(gate_rows, FS, split_axis=1, concat_axis=0, tiled=True)  17 us
    ppermute x4, waiting for transfers between devices, gather_around(): lower.append(lax.ppermute(lower[-1] if lower else x, axis, pairs))  16.5 us
  transfers between devices with their start and end apart: 15, of which 12 were waited for; matrix products, arithmetic and copies ran while one was open for 5% of the time, Pallas kernels for 0%

profile of v1, /device:TPU:34, one launch (start us, length us, event | category | flops | bytes accessed | tf_op | source)
XLA Modules:
  0.0 537.8 jit_solution(1482552838130556016)
XLA Ops:
  9.9 17.9 %collective-permute-start.2 = (bf16[64,1408]{1,0:T(8,128)(2,1)S(1)}, bf16[64,1408]{1,0:T(8,128)(2,1)S(1)}, u32[]{:S(2)}, u32[]{:S(2)}) collective-permute-start(bf16[64,1408]{1,0:T(8,128)(2,1)S(1)} %convert_element_type.62), channel_id=1, source_target_pairs={{1,0},{2,1},{3,2},{0,3},{5,4},{6,5},{7,6},{4,7},{9,8},{10,9},{11,1... | collective-permute-start | bytes 540680 | tf_op jit(solution)/shard_map/ppermute | solution.py:28
  31.2 6.6 %collective-permute-done.1 = bf16[64,1408]{1,0:T(8,128)(2,1)S(1)} collective-permute-done((bf16[64,1408]{1,0:T(8,128)(2,1)S(1)}, bf16[64,1408]{1,0:T(8,128)(2,1)S(1)}, u32[]{:S(2)}, u32[]{:S(2)}) %collective-permute-start.1) | collective-permute-done | bytes 180256 | tf_op jit(solution)/shard_map/ppermute | solution.py:26
  42.3 7.4 %all-to-all-start = ((bf16[64,32,176]{2,0,1:T(8,128)(2,1)}), bf16[64,32,176]{2,0,1:T(8,128)(2,1)S(1)}, u32[]{:S(2)}, u32[]{:S(2)}) async-start(bf16[64,32,176]{2,0,1:T(8,128)(2,1)} %copy.32), calls=%async_computation | async-start | bytes 2097152 | tf_op jit(solution)/shard_map/all_to_all | solution.py:74
  49.8 13.9 %all_gather.15 = bf16[64,5632]{1,0:T(8,128)(2,1)S(1)} all-gather(bf16[64,1408]{1,0:T(8,128)(2,1)S(1)} %convert_element_type.63), channel_id=1, replica_groups=mesh['grp'=2,'fs_0'=16,'fs_1'=2,'tp'=4] {'tp'}, dimensions={1}, use_global_device_ids=true | all-gather | bytes 901120 | tf_op jit(solution)/shard_map/all_gather | solution.py:70
  67.3 37.7 %all-to-all-done = bf16[64,32,176]{2,0,1:T(8,128)(2,1)S(1)} async-done(((bf16[64,32,176]{2,0,1:T(8,128)(2,1)}), bf16[64,32,176]{2,0,1:T(8,128)(2,1)S(1)}, u32[]{:S(2)}, u32[]{:S(2)}) %all-to-all-start) | async-done | bytes 720928 | tf_op jit(solution)/shard_map/all_to_all | solution.py:74
  105.0 4.8 all-to-all-start.1
  110.0 13.7 %all_gather.16 = bf16[176,2048]{1,0:T(8,128)(2,1)S(1)} all-gather(bf16[176,512]{1,0:T(8,128)(2,1)S(1)} %convert_element_type.65), channel_id=1, replica_groups=mesh['grp'=2,'fs_0'=16,'fs_1'=2,'tp'=4] {'tp'}, dimensions={1}, use_global_device_ids=true | all-gather | bytes 901120 | tf_op jit(solution)/shard_map/all_gather | solution.py:71
  127.7 37.9 %all-to-all-done.1 = bf16[64,32,176]{2,0,1:T(8,128)(2,1)S(1)} async-done(((bf16[64,32,176]{2,0,1:T(8,128)(2,1)}), bf16[64,32,176]{2,0,1:T(8,128)(2,1)S(1)}, u32[]{:S(2)}, u32[]{:S(2)}) %all-to-all-start.1) | async-done | bytes 720928 | tf_op jit(solution)/shard_map/all_to_all | solution.py:75
  165.6 7.0 %convolution_convert_fusion.1 = bf16[1024,2048]{1,0:T(8,128)(2,1)} fusion(bf16[176,2048]{1,0:T(8,128)(2,1)S(1)} %all_gather.16, bf16[2048,176]{1,0:T(8,128)(2,1)S(1)} %bitcast.74, bf16[1,1024,2048]{2,1,0:T(8,128)(2,1)} %param.8, f32[1024,176]{0,1:T(8,128)S(1)} %fusion.4), kind=kOutput, calls=%fused_computation.7 | convolution fusion | flops 1479573504 | bytes 10551296 | tf_op jit(solution)/shard_map/dot_general | solution.py:81
  172.5 4.7 copy.34
  177.4 12.8 %reduce-scatter.5.cloned.1.call-done = bf16[16,32,2048]{2,1,0:T(8,128)(2,1)} async-done(((bf16[32,32,2048]{2,1,0:T(8,128)(2,1)}), bf16[16,32,2048]{2,1,0:T(8,128)(2,1)}) %reduce-scatter.5.cloned.1.call-update) | async-done | bytes 2097168 | tf_op jit(solution)/shard_map/reduce_scatter | solution.py:40
  190.3 76.1 %reduce-scatter.7.cloned.1.call-done = bf16[1,32,2048]{2,1,0:T(8,128)(2,1)} async-done(((bf16[16,32,2048]{2,1,0:T(8,128)(2,1)}), bf16[1,32,2048]{2,1,0:T(8,128)(2,1)}) %reduce-scatter.7.cloned.1.call-update) | async-done | bytes 131088 | tf_op jit(solution)/shard_map/reduce_scatter | solution.py:40
  278.3 4.1 collective-permute-done.4
  289.0 9.7 %all-to-all-start.2 = ((bf16[64,32,176]{2,0,1:T(8,128)(2,1)}), bf16[64,32,176]{2,0,1:T(8,128)(2,1)S(1)}, u32[]{:S(2)}, u32[]{:S(2)}) async-start(bf16[64,32,176]{2,0,1:T(8,128)(2,1)} %copy.36), calls=%async_computation.4 | async-start | bytes 2097152 | tf_op jit(solution)/shard_map/all_to_all | solution.py:74
  298.6 14.5 %all_gather.18 = bf16[64,5632]{1,0:T(8,128)(2,1)} all-gather(bf16[64,1408]{1,0:T(8,128)(2,1)S(1)} %copy-done.5), channel_id=1, replica_groups=mesh['grp'=2,'fs_0'=16,'fs_1'=2,'tp'=4] {'tp'}, dimensions={1}, use_global_device_ids=true | all-gather | bytes 901120 | tf_op jit(solution)/shard_map/all_gather | solution.py:70
  319.7 43.4 %all-to-all-done.2 = bf16[64,32,176]{2,0,1:T(8,128)(2,1)S(1)} async-done(((bf16[64,32,176]{2,0,1:T(8,128)(2,1)}), bf16[64,32,176]{2,0,1:T(8,128)(2,1)S(1)}, u32[]{:S(2)}, u32[]{:S(2)}) %all-to-all-start.2) | async-done | bytes 720928 | tf_op jit(solution)/shard_map/all_to_all | solution.py:74
  363.1 5.5 %all-to-all-start.3 = ((bf16[64,32,176]{2,0,1:T(8,128)(2,1)}), bf16[64,32,176]{2,0,1:T(8,128)(2,1)}, u32[]{:S(2)}, u32[]{:S(2)}) async-start(bf16[64,32,176]{2,0,1:T(8,128)(2,1)} %copy.37), calls=%async_computation.5 | async-start | bytes 2097152 | tf_op jit(solution)/shard_map/all_to_all | solution.py:75
  368.8 14.7 %all_gather.19 = bf16[176,2048]{1,0:T(8,128)(2,1)} all-gather(bf16[176,512]{1,0:T(8,128)(2,1)S(1)} %convert_element_type.74), channel_id=1, replica_groups=mesh['grp'=2,'fs_0'=16,'fs_1'=2,'tp'=4] {'tp'}, dimensions={1}, use_global_device_ids=true | all-gather | bytes 901120 | tf_op jit(solution)/shard_map/all_gather | solution.py:71
  383.5 4.6 fusion.34
  388.1 36.0 %all-to-all-done.3 = bf16[64,32,176]{2,0,1:T(8,128)(2,1)} async-done(((bf16[64,32,176]{2,0,1:T(8,128)(2,1)}), bf16[64,32,176]{2,0,1:T(8,128)(2,1)}, u32[]{:S(2)}, u32[]{:S(2)}) %all-to-all-start.3) | async-done | bytes 720928 | tf_op jit(solution)/shard_map/all_to_all | solution.py:75
  424.1 7.7 %convolution_convert_fusion = bf16[1024,2048]{1,0:T(8,128)(2,1)} fusion(bf16[176,2048]{1,0:T(8,128)(2,1)} %all_gather.19, bf16[1024,2048]{1,0:T(8,128)(2,1)} %all-gather.2.cloned.1.call-done, bf16[2048,176]{1,0:T(8,128)(2,1)} %bitcast.24, f32[1024,176]{0,1:T(8,128)} %fusion.34), kind=kOutput, calls=%fused_computation.6 | convolution fusion | flops 1479573504 | bytes 10551296 | tf_op jit(solution)/shard_map/dot_general | solution.py:81
  431.7 4.7 copy.38
  436.6 12.8 %reduce-scatter.9.cloned.1.call-done = bf16[16,32,2048]{2,1,0:T(8,128)(2,1)} async-done(((bf16[32,32,2048]{2,1,0:T(8,128)(2,1)}), bf16[16,32,2048]{2,1,0:T(8,128)(2,1)}) %reduce-scatter.9.cloned.1.call-update) | async-done | bytes 2097168 | tf_op jit(solution)/shard_map/reduce_scatter | solution.py:40
  455.3 70.1 %reduce-scatter.11.cloned.1.call-done = bf16[1,32,2048]{2,1,0:T(8,128)(2,1)} async-done(((bf16[16,32,2048]{2,1,0:T(8,128)(2,1)}), bf16[1,32,2048]{2,1,0:T(8,128)(2,1)}) %reduce-scatter.11.cloned.1.call-update) | async-done | bytes 131088 | tf_op jit(solution)/shard_map/reduce_scatter | solution.py:40
  (89 shorter events, 55.4 us)
Async XLA Ops:
  8.2 23.0 %collective-permute-start = (bf16[64,1408]{1,0:T(8,128)(2,1)S(1)}, bf16[64,1408]{1,0:T(8,128)(2,1)S(1)}, u32[]{:S(2)}, u32[]{:S(2)}) collective-permute-start(bf16[64,1408]{1,0:T(8,128)(2,1)S(1)} %convert_element_type.62), channel_id=1, source_target_pairs={{0,1},{1,2},{2,3},{3,0},{4,5},{5,6},{6,7},{7,4},{8,9},{9,10},{10,1... | collective-permute-start | bytes 540680 | tf_op jit(solution)/shard_map/ppermute | solution.py:26
  9.9 21.3 %collective-permute-start.2 = (bf16[64,1408]{1,0:T(8,128)(2,1)S(1)}, bf16[64,1408]{1,0:T(8,128)(2,1)S(1)}, u32[]{:S(2)}, u32[]{:S(2)}) collective-permute-start(bf16[64,1408]{1,0:T(8,128)(2,1)S(1)} %convert_element_type.62), channel_id=1, source_target_pairs={{1,0},{2,1},{3,2},{0,3},{5,4},{6,5},{7,6},{4,7},{9,8},{10,9},{11,1... | collective-permute-start | bytes 540680 | tf_op jit(solution)/shard_map/ppermute | solution.py:28
  31.2 6.7 %collective-permute-start.1 = (bf16[64,1408]{1,0:T(8,128)(2,1)S(1)}, bf16[64,1408]{1,0:T(8,128)(2,1)S(1)}, u32[]{:S(2)}, u32[]{:S(2)}) collective-permute-start(bf16[64,1408]{1,0:T(8,128)(2,1)S(1)} %collective-permute-done), channel_id=1, source_target_pairs={{0,1},{1,2},{2,3},{3,0},{4,5},{5,6},{6,7},{7,4},{8,9},{9,10},{10,1... | collective-permute-start | bytes 540680 | tf_op jit(solution)/shard_map/ppermute | solution.py:26
  42.3 62.7 %all-to-all-start = ((bf16[64,32,176]{2,0,1:T(8,128)(2,1)}), bf16[64,32,176]{2,0,1:T(8,128)(2,1)S(1)}, u32[]{:S(2)}, u32[]{:S(2)}) async-start(bf16[64,32,176]{2,0,1:T(8,128)(2,1)} %copy.32), calls=%async_computation | async-start | bytes 2097152 | tf_op jit(solution)/shard_map/all_to_all | solution.py:74
  49.7 60.2 %copy-start.7 = (f32[176,512]{1,0:T(8,128)S(1)}, f32[176,512]{1,0:T(8,128)}, u32[]{:S(2)}) copy-start(f32[176,512]{1,0:T(8,128)} %param.11) | copy-start | bytes 1081348
  105.0 60.6 %all-to-all-start.1 = ((bf16[64,32,176]{2,0,1:T(8,128)(2,1)}), bf16[64,32,176]{2,0,1:T(8,128)(2,1)S(1)}, u32[]{:S(2)}, u32[]{:S(2)}) async-start(bf16[64,32,176]{2,0,1:T(8,128)(2,1)} %copy.33), calls=%async_computation.1 | async-start | bytes 2097152 | tf_op jit(solution)/shard_map/all_to_all | solution.py:75
  109.9 80.3 %reduce-scatter.5.cloned.1.call-start = ((), (), s32[]{:S(2)}) async-start(), calls=%async_computation.8 | async-start | bytes 6291456 | tf_op jit(solution)/shard_map/reduce_scatter | solution.py:40
  177.3 93.3 %copy-start.11 = (f32[2048]{0:T(1024)S(1)}, f32[2048]{0:T(1024)}, u32[]{:S(2)}) copy-start(f32[2048]{0:T(1024)} %param.12) | copy-start | bytes 24580
  177.3 93.4 %copy-start.9 = (f32[64,1408]{1,0:T(8,128)S(1)}, f32[64,1408]{1,0:T(8,128)}, u32[]{:S(2)}) copy-start(f32[64,1408]{1,0:T(8,128)} %param.13) | copy-start | bytes 1081348
  177.3 93.4 %copy-start.10 = (f32[64,1408]{1,0:T(8,128)S(1)}, f32[64,1408]{1,0:T(8,128)}, u32[]{:S(2)}) copy-start(f32[64,1408]{1,0:T(8,128)} %param.14) | copy-start | bytes 1081348
  177.3 89.1 %reduce-scatter.7.cloned.1.call-start = ((), (), s32[]{:S(2)}) async-start(), calls=%async_computation.9 | async-start | bytes 2228224 | tf_op jit(solution)/shard_map/reduce_scatter | solution.py:40
  190.2 193.2 %all-gather.2.cloned.1.call-start = ((), (), s32[]{:S(2)}) async-start(), calls=%async_computation.10 | async-start | bytes 4325376 | tf_op jit(solution)/shard_map/all_gather | solution.py:109
  271.4 5.5 %collective-permute-start.3 = (bf16[64,1408]{1,0:T(8,128)(2,1)S(1)}, bf16[64,1408]{1,0:T(8,128)(2,1)S(1)}, u32[]{:S(2)}, u32[]{:S(2)}) collective-permute-start(bf16[64,1408]{1,0:T(8,128)(2,1)S(1)} %get-tuple-element.21), channel_id=1, source_target_pairs={{0,1},{1,2},{2,3},{3,0},{4,5},{5,6},{6,7},{7,4},{8,9},{9,10},{10,1... | collective-permute-start | bytes 540680 | tf_op jit(solution)/shard_map/ppermute | solution.py:26
  272.8 5.5 %collective-permute-start.5 = (bf16[64,1408]{1,0:T(8,128)(2,1)S(1)}, bf16[64,1408]{1,0:T(8,128)(2,1)S(1)}, u32[]{:S(2)}, u32[]{:S(2)}) collective-permute-start(bf16[64,1408]{1,0:T(8,128)(2,1)S(1)} %get-tuple-element.21), channel_id=1, source_target_pairs={{1,0},{2,1},{3,2},{0,3},{5,4},{6,5},{7,6},{4,7},{9,8},{10,9},{11,1... | collective-permute-start | bytes 540680 | tf_op jit(solution)/shard_map/ppermute | solution.py:28
  276.9 5.5 %collective-permute-start.4 = (bf16[64,1408]{1,0:T(8,128)(2,1)S(1)}, bf16[64,1408]{1,0:T(8,128)(2,1)S(1)}, u32[]{:S(2)}, u32[]{:S(2)}) collective-permute-start(bf16[64,1408]{1,0:T(8,128)(2,1)S(1)} %collective-permute-done.3), channel_id=1, source_target_pairs={{0,1},{1,2},{2,3},{3,0},{4,5},{5,6},{6,7},{7,4},{8,9},{9,10},{10,1... | collective-permute-start | bytes 540680 | tf_op jit(solution)/shard_map/ppermute | solution.py:26
  289.0 74.2 %all-to-all-start.2 = ((bf16[64,32,176]{2,0,1:T(8,128)(2,1)}), bf16[64,32,176]{2,0,1:T(8,128)(2,1)S(1)}, u32[]{:S(2)}, u32[]{:S(2)}) async-start(bf16[64,32,176]{2,0,1:T(8,128)(2,1)} %copy.36), calls=%async_computation.4 | async-start | bytes 2097152 | tf_op jit(solution)/shard_map/all_to_all | solution.py:74
  363.1 60.9 %all-to-all-start.3 = ((bf16[64,32,176]{2,0,1:T(8,128)(2,1)}), bf16[64,32,176]{2,0,1:T(8,128)(2,1)}, u32[]{:S(2)}, u32[]{:S(2)}) async-start(bf16[64,32,176]{2,0,1:T(8,128)(2,1)} %copy.37), calls=%async_computation.5 | async-start | bytes 2097152 | tf_op jit(solution)/shard_map/all_to_all | solution.py:75
  368.7 80.7 %reduce-scatter.9.cloned.1.call-start = ((), (), s32[]{:S(2)}) async-start(), calls=%async_computation.11 | async-start | bytes 6291456 | tf_op jit(solution)/shard_map/reduce_scatter | solution.py:40
  436.5 89.0 %reduce-scatter.11.cloned.1.call-start = ((), (), s32[]{:S(2)}) async-start(), calls=%async_computation.12 | async-start | bytes 2228224 | tf_op jit(solution)/shard_map/reduce_scatter | solution.py:40
  449.4 76.1 %copy-start.4 = (bf16[32,2048]{1,0:T(8,128)(2,1)S(1)}, bf16[32,2048]{1,0:T(8,128)(2,1)}, u32[]{:S(2)}) copy-start(bf16[32,2048]{1,0:T(8,128)(2,1)} %multiply_convert_fusion.3) | copy-start | bytes 393220
  449.5 78.2 %copy-start.3 = (bf16[1,32,2048]{2,1,0:T(8,128)(2,1)S(1)}, bf16[1,32,2048]{2,1,0:T(8,128)(2,1)}, u32[]{:S(2)}) copy-start(bf16[1,32,2048]{2,1,0:T(8,128)(2,1)} %reduce-scatter.7.cloned.1.call-done) | copy-start | bytes 393220
  449.5 78.2 %copy-start.13 = (f32[32]{0:T(128)S(1)}, f32[32]{0:T(128)}, u32[]{:S(2)}) copy-start(f32[32]{0:T(128)} %copy-done.12) | copy-start | bytes 388
  452.9 76.6 %copy-start.1 = (bf16[176,2048]{1,0:T(8,128)(2,1)S(1)}, bf16[176,2048]{1,0:T(8,128)(2,1)}, u32[]{:S(2)}) copy-start(bf16[176,2048]{1,0:T(8,128)(2,1)} %copy-done) | copy-start | bytes 2162692
  454.1 76.2 %copy-start.2 = (bf16[176,2048]{1,0:T(8,128)(2,1)S(1)}, bf16[176,2048]{1,0:T(8,128)(2,1)}, u32[]{:S(2)}) copy-start(bf16[176,2048]{1,0:T(8,128)(2,1)} %all_gather.19) | copy-start | bytes 2162692
  (5 other events, 143.9 us)
Sparse Core Ops, SparseCore 0:
  177.5 12.6 reduce-scatter.4
  192.7 73.6 reduce-scatter.6
  270.7 98.1 all-gather.1
  436.6 12.7 reduce-scatter.8
  451.8 73.6 reduce-scatter.10
